TPU v7x, 512 devices: a whole 4x8x8 slice. The times are simulated.
512 devices in a mesh: ep: 32 (over z, x), tp: 16 (over y, core).
Axes of the slice: x: 4, y: 8, z: 8, core: 2. Of those that a mesh axis runs over, the one named last changes fastest.
Arguments:
- queries: bfloat16 [8192, 2048], P('ep', 'tp'), may hold values from -9 to 9
- key_rows: bfloat16 [8192, 2048], P('ep', 'tp'), may hold values from -9 to 9
- values: bfloat16 [8192, 2048], P('ep', 'tp'), may hold values from -6 to 6
- second_scale: float32 [16], P('tp'), may hold values from 0.3 to 0.8
- head_gain: float32 [128], replicated, may hold values from 0.1 to 1.9
- out_weight: bfloat16 [2048, 2048], P(None, 'tp'), may hold values from -0.125 to 0.125
- routed_in: bfloat16 [8192, 2048], P('ep'), may hold values from -6 to 6
- routed_gain: float32 [2048], replicated, may hold values from 0.1 to 1.9
- expert_ids: int32 [8192, 2], P('ep'), may hold values from 0 to 31, all different within a row; in each aligned block of 256 rows (0 to 255, 256 to 511, ...) at most 32 rows name the same one
- group_logits: float32 [8192, 8], P('ep'), may hold values from -6 to 6
- inner_logits: float32 [8192, 2], P('ep'), may hold values from -6 to 6
- gate_weight: bfloat16 [32, 2048, 4096], P('ep', None, 'tp'), may hold values from -0.125 to 0.125
- up_weight: bfloat16 [32, 2048, 4096], P('ep', None, 'tp'), may hold values from -0.125 to 0.125
- down_weight: bfloat16 [32, 4096, 2048], P('ep', 'tp'), may hold values from -0.09375 to 0.09375
Outputs:
- mixer_out: bfloat16 [8192, 2048], P('ep', 'tp')
- routed_out: bfloat16 [8192, 2048], P('ep', 'tp')
Inputs may be any that keep to these rules, and one draw needn't show every extreme that they name: `expert_ids`: the two ids of a row differ. In the rows of one device (aligned blocks of 256 rows) no expert is named by more than 32 rows, a bound that some block reaches.
All inputs are finite; a program needn't handle non-finite values.
Results may differ from a plain program's by a relative error of at most 0.018.
Values may be sent and summed in bfloat16 or wider, within the bound.
A program may use at most 128 MiB of HBM per device.

v0:
```python
import math
import jax
import jax.numpy as jnp
from jax import lax
from jax.sharding import Mesh
from jax.sharding import PartitionSpec as P

GROUP_SIZE = 4
EP = ("ep_0", "ep_1")
EPSILON = 1e-05
LOWEST = -1e30


def whole_of(array, axes, dim):
    if not axes:
        return array
    nearer = lax.all_gather(array, axes[-1], axis=dim, tiled=True)
    return whole_of(nearer, axes[:-1], dim)


def token_mixer(queries, key_rows, values, second_scale, head_gain, out_weight):
    row_count = queries.shape[0]
    local_heads = second_scale.shape[0]
    qk_size = queries.shape[1] // (2 * local_heads)
    value_size = values.shape[1] // local_heads
    first_pos = lax.axis_index(EP) * row_count
    query_pos = first_pos + jnp.arange(row_count, dtype=jnp.int32)
    last_pos = first_pos + row_count - 1
    query_four = queries.reshape(row_count, local_heads, 2, qk_size)
    score_scale = qk_size ** (-0.5)
    initial = (
        jnp.full((row_count, local_heads, 2), LOWEST, jnp.float32),
        jnp.zeros((row_count, local_heads, 2), jnp.float32),
        jnp.zeros((row_count, local_heads, 2, value_size), jnp.float32),
    )
    state_now = initial
    key_piece = whole_of(key_rows, EP, 0)
    value_piece = whole_of(values, EP, 0)
    piece_count = key_piece.shape[0]
    block_width = math.gcd(piece_count, 512)
    blocks = piece_count // block_width
    key_blocks = key_piece.reshape(blocks, block_width, local_heads, 2, qk_size)
    value_blocks = value_piece.reshape(blocks, block_width, local_heads, value_size)

    def update(state_inner, block_index):
        key_start = block_index * block_width

        def attend(inner_state):
            running_max, denominator, weighted = inner_state
            scores = (
                jnp.einsum(
                    "qhmd,khmd->qhmk",
                    query_four,
                    key_blocks[block_index],
                    preferred_element_type=jnp.float32,
                )
                * score_scale
            )
            key_pos = key_start + jnp.arange(block_width, dtype=jnp.int32)
            visible = (query_pos[:, None] >= key_pos[None, :])[:, None, None, :]
            scores = jnp.where(visible, scores, LOWEST)
            new_max = jnp.maximum(running_max, jnp.max(scores, axis=-1))
            exp_terms = jnp.where(visible, jnp.exp(scores - new_max[..., None]), 0.0)
            factor = jnp.exp(running_max - new_max)
            denominator = denominator * factor + jnp.sum(exp_terms, axis=-1)
            weighted = weighted * factor[..., None] + jnp.einsum(
                "qhmk,khe->qhme",
                exp_terms.astype(jnp.bfloat16),
                value_blocks[block_index],
                preferred_element_type=jnp.float32,
            )
            return (new_max, denominator, weighted)

        return (
            lax.cond(key_start <= last_pos, attend, lambda inner_state: inner_state, state_inner),
            None,
        )

    state_now, _ = lax.scan(update, state_now, jnp.arange(blocks, dtype=jnp.int32))
    running_max, denominator, weighted = state_now
    mapped = weighted / denominator[..., None]
    difference = mapped[:, :, 0] - second_scale[None, :, None] * mapped[:, :, 1]
    inv_norm = lax.rsqrt(jnp.mean(difference * difference, axis=-1, keepdims=True) + EPSILON)
    head_out = (
        (difference * inv_norm * head_gain)
        .astype(jnp.bfloat16)
        .reshape(row_count, local_heads * value_size)
    )
    mixed = jnp.dot(
        lax.all_gather(head_out, "tp", axis=1, tiled=True),
        out_weight,
        preferred_element_type=jnp.float32,
    )
    return mixed.astype(jnp.bfloat16)


def expert_block(
    routed_in,
    routed_gain,
    expert_ids,
    group_logits,
    inner_logits,
    gate_weight,
    up_weight,
    down_weight,
):
    token_count = routed_in.shape[0]
    chosen = expert_ids.shape[1]
    ep_size = lax.axis_size(EP)
    capacity = 2 * chosen * token_count // ep_size
    source = routed_in.astype(jnp.float32)
    normed = (
        source
        * lax.rsqrt(jnp.mean(source * source, axis=-1, keepdims=True) + EPSILON)
        * routed_gain
    ).astype(jnp.bfloat16)
    flat_ids = expert_ids.reshape(-1)
    picked = (flat_ids[:, None] == jnp.arange(ep_size, dtype=jnp.int32)[None, :]).astype(jnp.int32)
    slot_index = jnp.sum(jnp.cumsum(picked, axis=0) * picked, axis=1) - 1
    place_index = flat_ids * capacity + slot_index
    owner_row = jnp.arange(token_count * chosen, dtype=jnp.int32) // chosen
    slot_rows = jnp.zeros((ep_size * capacity,), jnp.int32).at[place_index].set(owner_row)
    outgoing = normed[slot_rows].reshape(ep_size, capacity, normed.shape[1])
    gate_local = gate_weight[0]
    up_local = up_weight[0]
    down_local = down_weight[0]
    columns = outgoing.shape[2] // lax.axis_size("tp")
    own_columns = lax.dynamic_slice_in_dim(outgoing, lax.axis_index("tp") * columns, columns, 2)
    arrived = lax.all_to_all(own_columns, EP, split_axis=0, concat_axis=0, tiled=True)
    experts_arrived = lax.all_gather(arrived, "tp", axis=2, tiled=True)
    stacked = experts_arrived.reshape(-1, experts_arrived.shape[2])
    gate_act = jnp.dot(stacked, gate_local, preferred_element_type=jnp.float32)
    up_act = jnp.dot(stacked, up_local, preferred_element_type=jnp.float32)
    hidden = (jax.nn.silu(gate_act) * up_act).astype(jnp.bfloat16)
    partial_value = jnp.dot(hidden, down_local, preferred_element_type=jnp.float32)
    partial_value = partial_value.reshape(
        experts_arrived.shape[0], experts_arrived.shape[1], partial_value.shape[1]
    )
    answered = lax.psum_scatter(
        partial_value.astype(jnp.bfloat16), "tp", scatter_dimension=2, tiled=True
    )
    returned = lax.all_to_all(answered, EP, split_axis=0, concat_axis=0, tiled=True)
    pair_out = returned.reshape(ep_size * capacity, returned.shape[2])[place_index]
    pair_out = pair_out.reshape(token_count, chosen, returned.shape[2])
    group_prob = jax.nn.softmax(group_logits, axis=-1)
    member = (
        expert_ids[..., None] // GROUP_SIZE == jnp.arange(group_logits.shape[1], dtype=jnp.int32)
    ).astype(jnp.float32)
    group_pick = jnp.sum(group_prob[:, None, :] * member, axis=-1)
    route_weight = group_pick * jax.nn.softmax(inner_logits, axis=-1)
    return jnp.sum(route_weight[..., None] * pair_out.astype(jnp.float32), axis=1).astype(
        jnp.bfloat16
    )


def local(
    queries,
    key_rows,
    values,
    second_scale,
    head_gain,
    out_weight,
    routed_in,
    routed_gain,
    expert_ids,
    group_logits,
    inner_logits,
    gate_weight,
    up_weight,
    down_weight,
):
    mixer_out = token_mixer(queries, key_rows, values, second_scale, head_gain, out_weight)
    routed_out = expert_block(
        routed_in,
        routed_gain,
        expert_ids,
        group_logits,
        inner_logits,
        gate_weight,
        up_weight,
        down_weight,
    )
    return (mixer_out, routed_out)


def solution(mesh):
    finer = Mesh(mesh.devices.reshape(8, 4, mesh.shape["tp"]), ("ep_0", "ep_1", "tp"))
    placed = (
        P(EP, "tp"),
        P(EP, "tp"),
        P(EP, "tp"),
        P("tp"),
        P(),
        P(None, "tp"),
        P(EP, None),
        P(),
        P(EP, None),
        P(EP, None),
        P(EP, None),
        P(EP, None, "tp"),
        P(EP, None, "tp"),
        P(EP, "tp", None),
    )
    return jax.shard_map(
        local, mesh=finer, in_specs=placed, out_specs=(P(EP, "tp"), P(EP, "tp")), check_vma=False
    )
```

profile of v0, /device:TPU:1, one launch (start us, length us, event | category | flops | bytes accessed | tf_op | source)
XLA Modules:
  0.0 325.3 jit_solution(6230517476498490236)
XLA Ops:
  11.0 2.4 scatter_custom_fusion
  13.5 1.5 fusion.21
  15.0 1.5 fusion.23
  16.6 6.0 %gather_fusion = bf16[1024,2048]{1,0:T(8,128)(2,1)} fusion(bf16[256,2048]{1,0:T(8,128)(2,1)S(1)} %fusion.23, s32[1024]{0:T(1024)S(1)} %fusion.38), kind=kCustom, calls=%fused_computation | custom fusion | bytes 8392704 | tf_op jit(solution)/shard_map/gather | solution.py:123
  23.5 24.9 %all_to_all.10 = bf16[32,32,128]{2,1,0:T(8,128)(2,1)} all-to-all(bf16[32,32,128]{2,1,0:T(8,128)(2,1)S(1)} %constant_dynamic-slice_fusion), channel_id=1, replica_groups=mesh['ep_0'=8,'ep_1'=4,'tp'=16] {'ep_0','ep_1'}, dimensions={0} | all-to-all | bytes 524288 | tf_op jit(solution)/shard_map/all_to_all | solution.py:129
  48.6 10.7 %all_gather.18 = bf16[1024,128]{1,0:T(8,128)(2,1)} all-gather(bf16[256,128]{1,0:T(8,128)(2,1)S(1)} %copy-done.3), channel_id=1, replica_groups=mesh['ep_0'=8,'ep_1'=4,'tp'=16] {'ep_1'}, dimensions={0}, use_global_device_ids=true | all-gather | bytes 327680 | tf_op jit(solution)/shard_map/all_gather | solution.py:17
  59.4 11.1 %all_gather.20 = bf16[1024,128]{1,0:T(8,128)(2,1)} all-gather(bf16[256,128]{1,0:T(8,128)(2,1)S(1)} %copy-done.4), channel_id=1, replica_groups=mesh['ep_0'=8,'ep_1'=4,'tp'=16] {'ep_1'}, dimensions={0}, use_global_device_ids=true | all-gather | bytes 327680 | tf_op jit(solution)/shard_map/all_gather | solution.py:17
  70.6 28.3 %all-gather.11.cloned.1.call-done = bf16[32,32,2048]{2,1,0:T(8,128)(2,1)} async-done(((bf16[32,32,128]{2,1,0:T(8,128)(2,1)}), bf16[32,32,2048]{2,1,0:T(8,128)(2,1)}) %all-gather.11.cloned.1.call-update) | async-done | bytes 4194320 | tf_op jit(solution)/shard_map/all_gather | solution.py:130
  98.8 3.6 %fusion.27 = f32[1024,256]{1,0:T(8,128)S(1)} fusion(bf16[1024,2048]{1,0:T(8,128)(2,1)} %bitcast.107, bf16[1,2048,256]{2,1,0:T(8,128)(2,1)S(1)} %copy-done.9), kind=kOutput, calls=%fused_computation.42 | convolution fusion | flops 1073741824 | bytes 6291456 | tf_op jit(solution)/shard_map/dot_general | solution.py:132
  103.7 3.2 convolution_convert_fusion
  106.9 23.0 %copy.58 = bf16[32,32,2048]{1,0,2:T(8,128)(2,1)} copy(bf16[32,32,2048]{2,1,0:T(8,128)(2,1)} %convolution_convert_fusion) | data formatting | bytes 8388608
  130.0 23.3 %reshape.280 = bf16[2048,1024]{1,0:T(8,128)(2,1)} reshape(bf16[2048,32,32]{2,1,0:T(8,128)(2,1)} %bitcast.93) | data formatting | bytes 8388608
  154.9 8.2 %reshape.279 = bf16[16,512,1,2,64]{4,3,1,0,2:T(2,128)(2,1)} reshape(bf16[8192,128]{1,0:T(8,128)(2,1)} %all-gather.5.cloned.1.call-done) | data formatting | bytes 4194304 | tf_op jit(solution)/shard_map/reshape | solution.py:42
  163.1 9.1 %copy.48 = bf16[16,512,1,2,64]{1,4,3,2,0:T(8,128)(2,1)S(1)} copy(bf16[16,512,1,2,64]{4,3,1,0,2:T(2,128)(2,1)} %reshape.279) | data formatting | bytes 4194304
  172.2 10.3 %all-gather.7.cloned.1.call-done = bf16[8192,128]{1,0:T(8,128)(2,1)} async-done(((bf16[1024,128]{1,0:T(8,128)(2,1)}), bf16[8192,128]{1,0:T(8,128)(2,1)}) %all-gather.7.cloned.1.call-update) | async-done | bytes 2097168 | tf_op jit(solution)/shard_map/all_gather | solution.py:17
  182.6 3.9 %copy.49 = bf16[16,512,1,128]{1,3,2,0:T(8,128)(2,1)} copy(bf16[16,512,1,128]{3,1,0,2:T(8,128)(2,1)} %bitcast.98) | data formatting | bytes 4194304
  186.6 24.3 %while.15 = (s32[]{:T(128)}, f32[256,1,2]{0,2,1:T(2,128)S(1)}, f32[256,1,2]{0,2,1:T(2,128)S(1)}, f32[256,1,2,128]{0,3,2,1:T(8,128)S(1)}, s32[16]{0:T(128)S(1)}, ...) while((s32[]{:T(128)}, f32[256,1,2]{0,2,1:T(2,128)S(1)}, ...), condition=%wide.region_5.6_spmd.clone, body=%wide.region_0.5_spmd.clone.sunk | while | flops 103287040 | bytes 4563285 | solution.py:79
  187.8 4.0 %conditional.3 = ((f32[256,1,2]{0,2,1:T(2,128)S(1)}, f32[256,1,2]{0,2,1:T(2,128)S(1)}, f32[256,1,2,128]{0,3,2,1:T(8,128)S(1)})) conditional(s32[]{:T(128)} %convert_element_type.73, (f32[256,1,2]{0,2,1:T(2,128)S(1)}, f32[256,1,2]{0,2,1:T(2,128)S(1)}, f32[256,1,2,128]{0,3,2,1:T(8,128)S(1)}) %tuple.42, (s32[]{:T(128)}, s32[]{:T(128)}, s32[]{:T(128)}, ...), branch_computations={%region_1.1_spmd, %region_2.4_spmd} | conditional | flops 103287040 | bytes 4562002 | solution.py:75
  211.9 39.5 %reduce-scatter.4.cloned.1.call-done = bf16[128,1024]{1,0:T(8,128)(2,1)} async-done(((bf16[2048,1024]{1,0:T(8,128)(2,1)}), bf16[128,1024]{1,0:T(8,128)(2,1)}) %reduce-scatter.4.cloned.1.call-update) | async-done | bytes 262160
  251.4 1.8 reshape.281
  253.3 1.8 copy.59
  255.1 25.9 %all-to-all-start.1 = ((bf16[32,32,128]{2,1,0:T(8,128)(2,1)}), bf16[32,32,128]{2,1,0:T(8,128)(2,1)S(1)}, u32[]{:S(2)}, u32[]{:S(2)}) async-start(bf16[32,32,128]{2,1,0:T(8,128)(2,1)} %copy.59), calls=%async_computation.1 | async-start | bytes 524288 | tf_op jit(solution)/shard_map/all_to_all | solution.py:142
  281.1 32.9 %all-gather.9.cloned.1.call-done = bf16[256,2048]{0,1:T(8,128)(2,1)} async-done(((bf16[256,128]{0,1:T(8,128)(2,1)}), bf16[256,2048]{0,1:T(8,128)(2,1)}) %all-gather.9.cloned.1.call-update) | async-done | bytes 1048592 | tf_op jit(solution)/shard_map/all_gather | solution.py:90
  314.0 2.3 convolution_convert_fusion.1
  (129 shorter events, 22.5 us)
Async XLA Ops:
  7.2 96.6 %copy-start = (bf16[1,256,2048]{2,1,0:T(8,128)(2,1)S(1)}, bf16[1,256,2048]{2,1,0:T(8,128)(2,1)}, u32[]{:S(2)}) copy-start(bf16[1,256,2048]{2,1,0:T(8,128)(2,1)} %param.31) | copy-start | bytes 3145732
  7.2 91.6 %all-gather.11.cloned.1.call-start = ((), (), s32[]{:S(2)}) async-start(), calls=%async_computation.6 | async-start | bytes 4456448 | tf_op jit(solution)/shard_map/all_gather | solution.py:130
  16.5 32.0 %copy-start.3 = (bf16[256,128]{1,0:T(8,128)(2,1)S(1)}, bf16[256,128]{1,0:T(8,128)(2,1)}, u32[]{:S(2)}) copy-start(bf16[256,128]{1,0:T(8,128)(2,1)} %param.19) | copy-start | bytes 196612
  16.5 42.8 %copy-start.4 = (bf16[256,128]{1,0:T(8,128)(2,1)S(1)}, bf16[256,128]{1,0:T(8,128)(2,1)}, u32[]{:S(2)}) copy-start(bf16[256,128]{1,0:T(8,128)(2,1)} %param.20) | copy-start | bytes 196612
  16.5 82.3 %copy-start.9 = (bf16[1,2048,256]{2,1,0:T(8,128)(2,1)S(1)}, bf16[1,2048,256]{2,1,0:T(8,128)(2,1)}, u32[]{:S(2)}) copy-start(bf16[1,2048,256]{2,1,0:T(8,128)(2,1)} %param.29) | copy-start | bytes 3145732
  48.5 106.4 %all-gather.5.cloned.1.call-start = ((), (), s32[]{:S(2)}) async-start(), calls=%async_computation.3 | async-start | bytes 2359296 | tf_op jit(solution)/shard_map/all_gather | solution.py:17
  59.3 43.2 %copy-start.10 = (bf16[1,2048,256]{2,1,0:T(8,128)(2,1)S(1)}, bf16[1,2048,256]{2,1,0:T(8,128)(2,1)}, u32[]{:S(2)}) copy-start(bf16[1,2048,256]{2,1,0:T(8,128)(2,1)} %param.30) | copy-start | bytes 3145732
  59.3 123.3 %all-gather.7.cloned.1.call-start = ((), (), s32[]{:S(2)}) async-start(), calls=%async_computation.4 | async-start | bytes 2359296 | tf_op jit(solution)/shard_map/all_gather | solution.py:17
  70.5 180.9 %reduce-scatter.4.cloned.1.call-start = ((), (), s32[]{:S(2)}) async-start(), calls=%async_computation.7 | async-start | bytes 4456448
  98.8 3.6 %copy-start.8 = (bf16[32,32,2048]{2,1,0:T(8,128)(2,1)S(1)}, bf16[32,32,2048]{2,1,0:T(8,128)(2,1)}, u32[]{:S(2)}) copy-start(bf16[32,32,2048]{2,1,0:T(8,128)(2,1)} %all-gather.11.cloned.1.call-done) | copy-start | bytes 12582916
  153.3 0.8 copy-start.5
  153.3 160.7 %all-gather.9.cloned.1.call-start = ((), (), s32[]{:S(2)}) async-start(), calls=%async_computation.5 | async-start | bytes 1114112 | tf_op jit(solution)/shard_map/all_gather | solution.py:90
  186.5 24.4 %copy-start.7 = (f32[128]{0:T(128)S(1)}, f32[128]{0:T(128)}, u32[]{:S(2)}) copy-start(f32[128]{0:T(128)} %param.22) | copy-start | bytes 1540
  186.6 25.2 %copy-start.2 = (f32[256,8]{0,1:T(8,128)S(1)}, f32[256,8]{0,1:T(8,128)}, u32[]{:S(2)}) copy-start(f32[256,8]{0,1:T(8,128)} %param.27) | copy-start | bytes 24580
  186.6 25.2 %copy-start.6 = (f32[256,2]{0,1:T(2,128)S(1)}, f32[256,2]{0,1:T(2,128)}, u32[]{:S(2)}) copy-start(f32[256,2]{0,1:T(2,128)} %param.28) | copy-start | bytes 6148
  210.9 103.1 %copy-start.1 = (bf16[2048,128]{1,0:T(8,128)(2,1)S(1)}, bf16[2048,128]{1,0:T(8,128)(2,1)}, u32[]{:S(2)}) copy-start(bf16[2048,128]{1,0:T(8,128)(2,1)} %param.23) | copy-start | bytes 1572868
  255.1 61.3 %all-to-all-start.1 = ((bf16[32,32,128]{2,1,0:T(8,128)(2,1)}), bf16[32,32,128]{2,1,0:T(8,128)(2,1)S(1)}, u32[]{:S(2)}, u32[]{:S(2)}) async-start(bf16[32,32,128]{2,1,0:T(8,128)(2,1)} %copy.59), calls=%async_computation.1 | async-start | bytes 524288 | tf_op jit(solution)/shard_map/all_to_all | solution.py:142
Sparse Core Ops, SparseCore 0:
  48.6 50.1 all-gather.10
  100.9 37.4 all-gather.4
  140.5 42.0 all-gather.6
  185.3 66.1 reduce-scatter.3
  254.0 59.9 all-gather.8
where the time goes:
time: 328 us; the launch traced here: 325 us
  waiting for transfers between devices  111 us (34%)
  local copies, waits for them, and re-layouts  94.1 us (29%)
  blocking collectives  46.8 us (14%)
  starting transfers between devices  26.3 us (8%)
  between operations  14.8 us (5%)
  loops' own time  12.6 us (4%)
  matrix products  12.1 us (4%)
  other arithmetic  7.48 us (2%)
    unnamed x30, local copies, waits for them, and re-layouts  64.6 us
    unnamed x6, waiting for transfers between devices  39.6 us
    all_gather x1, waiting for transfers between devices, token_mixer(): lax.all_gather(head_out, 'tp', axis=1, tiled=True)  32.9 us
    all_gather x1, waiting for transfers between devices, expert_block(): experts_arrived = lax.all_gather(arrived, 'tp', axis=2, tiled=True)  28.3 us
    all_to_all x1, starting transfers between devices, expert_block(): lax.all_to_all(answered, EP, split_axis=0, concat_axis=0, tiled=True)  25.9 us
    all_to_all x1, blocking collectives, expert_block(): lax.all_to_all(own_columns, EP, split_axis=0, concat_axis=0, tiled=True)  24.9 us
    all_gather x2, blocking collectives, whole_of(): nearer = lax.all_gather(array, axes[-1], axis=dim, tiled=True)  21.8 us
    another operation x1, loops' own time, token_mixer(): lax.scan(update, state_now, jnp.arange(blocks, dtype=jnp.int32))  10.6 us
  transfers between devices with their start and end apart: 6, of which 4 were waited for; matrix products, arithmetic and copies ran while one was open for 29% of the time, Pallas kernels for 0%

commit v1 on v0

--- a/solution.py
+++ b/solution.py
@@ -9,6 +9,11 @@
 EP = ("ep_0", "ep_1")
 EPSILON = 1e-05
 LOWEST = -1e30
+
+
+def all_by_exchange(value, axis, along):
+    sent = jnp.stack([value] * lax.axis_size(axis))
+    return jnp.concatenate(lax.all_to_all(sent, axis, 0, 0), axis=along)
 
 
 def whole_of(array, axes, dim):
@@ -87,9 +92,7 @@
         .reshape(row_count, local_heads * value_size)
     )
     mixed = jnp.dot(
-        lax.all_gather(head_out, "tp", axis=1, tiled=True),
-        out_weight,
-        preferred_element_type=jnp.float32,
+        all_by_exchange(head_out, "tp", 1), out_weight, preferred_element_type=jnp.float32
     )
     return mixed.astype(jnp.bfloat16)
 

time: 328 us -> 341 us (1.040)
  starting transfers between devices: 26.3 us -> 56.1 us
  waiting for transfers between devices: 111 us -> 94.2 us
    all_gather x1 -> x0, waiting for transfers between devices: 32.9 us -> none  [token_mixer(): lax.all_gather(head_out, 'tp', axis=1, tiled=True)]
    all_to_all x1, starting transfers between devices: 25.9 us -> 44.5 us  [expert_block(): lax.all_to_all(answered, EP, split_axis=0, concat_axis=0, tiled=True)]
    all_to_all x0 -> x1, starting transfers between devices: none -> 11.2 us  [all_by_exchange(): return jnp.concatenate(lax.all_to_all(sent, axis, 0, 0), axis=along)]
    all_to_all x1, waiting for transfers between devices: 0.01 us -> 10.3 us  [expert_block(): lax.all_to_all(answered, EP, split_axis=0, concat_axis=0, tiled=True)]
    unnamed x6 -> x5, waiting for transfers between devices: 39.6 us -> 45.3 us
    unnamed x30 -> x28, local copies, waits for them, and re-layouts: 64.6 us -> 64.8 us
  transfers between devices with their start and end apart: 6 -> 6, of which waited for: 4 -> 4; matrix products, arithmetic and copies ran while one was open for 29% -> 28% of each run, Pallas kernels for 0% -> 0%
where the time goes in v1:
time: 341 us; the launch traced here: 339 us
  local copies, waits for them, and re-layouts  95.4 us (28%)
  waiting for transfers between devices  94.2 us (28%)
  starting transfers between devices  56.1 us (16%)
  blocking collectives  46.8 us (14%)
  between operations  14.8 us (4%)
  loops' own time  12.6 us (4%)
  matrix products  11.9 us (3%)
  other arithmetic  6.86 us (2%)
    unnamed x28, local copies, waits for them, and re-layouts  64.8 us
    unnamed x5, waiting for transfers between devices  45.3 us
    all_to_all x1, starting transfers between devices, expert_block(): lax.all_to_all(answered, EP, split_axis=0, concat_axis=0, tiled=True)  44.5 us
    all_gather x1, waiting for transfers between devices, expert_block(): experts_arrived = lax.all_gather(arrived, 'tp', axis=2, tiled=True)  28.1 us
    all_to_all x1, blocking collectives, expert_block(): lax.all_to_all(own_columns, EP, split_axis=0, concat_axis=0, tiled=True)  24.9 us
    all_gather x2, blocking collectives, whole_of(): nearer = lax.all_gather(array, axes[-1], axis=dim, tiled=True)  21.8 us
    all_to_all x1, starting transfers between devices, all_by_exchange(): return jnp.concatenate(lax.all_to_all(sent, axis, 0, 0), axis=along)  11.2 us
    another operation x1, loops' own time, token_mixer(): lax.scan(update, state_now, jnp.arange(blocks, dtype=jnp.int32))  10.6 us
  transfers between devices with their start and end apart: 6, of which 4 were waited for; matrix products, arithmetic and copies ran while one was open for 28% of the time, Pallas kernels for 0%

profile of v1, /device:TPU:1, one launch (start us, length us, event | category | flops | bytes accessed | tf_op | source)
XLA Modules:
  0.0 338.6 jit_solution(8997258510130477030)
XLA Ops:
  11.0 2.4 scatter_custom_fusion
  15.0 1.5 fusion.23
  16.6 6.0 %gather_fusion = bf16[1024,2048]{1,0:T(8,128)(2,1)} fusion(bf16[256,2048]{1,0:T(8,128)(2,1)S(1)} %fusion.23, s32[1024]{0:T(1024)S(1)} %fusion.38), kind=kCustom, calls=%fused_computation | custom fusion | bytes 8392704 | tf_op jit(solution)/shard_map/gather | solution.py:126
  23.5 24.9 %all_to_all.15 = bf16[32,32,128]{2,1,0:T(8,128)(2,1)} all-to-all(bf16[32,32,128]{2,1,0:T(8,128)(2,1)S(1)} %constant_dynamic-slice_fusion), channel_id=1, replica_groups=mesh['ep_0'=8,'ep_1'=4,'tp'=16] {'ep_0','ep_1'}, dimensions={0} | all-to-all | bytes 524288 | tf_op jit(solution)/shard_map/all_to_all | solution.py:132
  48.6 10.7 %all_gather.15 = bf16[1024,128]{1,0:T(8,128)(2,1)} all-gather(bf16[256,128]{1,0:T(8,128)(2,1)S(1)} %copy-done.2), channel_id=1, replica_groups=mesh['ep_0'=8,'ep_1'=4,'tp'=16] {'ep_1'}, dimensions={0}, use_global_device_ids=true | all-gather | bytes 327680 | tf_op jit(solution)/shard_map/all_gather | solution.py:22
  59.4 11.1 %all_gather.17 = bf16[1024,128]{1,0:T(8,128)(2,1)} all-gather(bf16[256,128]{1,0:T(8,128)(2,1)S(1)} %copy-done.3), channel_id=1, replica_groups=mesh['ep_0'=8,'ep_1'=4,'tp'=16] {'ep_1'}, dimensions={0}, use_global_device_ids=true | all-gather | bytes 327680 | tf_op jit(solution)/shard_map/all_gather | solution.py:22
  70.7 28.1 %all-gather.8.cloned.1.call-done = bf16[32,32,2048]{2,1,0:T(8,128)(2,1)} async-done(((bf16[32,32,128]{2,1,0:T(8,128)(2,1)}), bf16[32,32,2048]{2,1,0:T(8,128)(2,1)}) %all-gather.8.cloned.1.call-update) | async-done | bytes 4194320 | tf_op jit(solution)/shard_map/all_gather | solution.py:133
  98.8 3.6 %fusion.27 = f32[1024,256]{1,0:T(8,128)S(1)} fusion(bf16[1024,2048]{1,0:T(8,128)(2,1)} %bitcast.111, bf16[1,2048,256]{2,1,0:T(8,128)(2,1)S(1)} %copy-done.8), kind=kOutput, calls=%fused_computation.42 | convolution fusion | flops 1073741824 | bytes 6291456 | tf_op jit(solution)/shard_map/dot_general | solution.py:135
  103.7 3.2 convolution_convert_fusion
  106.9 23.0 %copy.59 = bf16[32,32,2048]{1,0,2:T(8,128)(2,1)} copy(bf16[32,32,2048]{2,1,0:T(8,128)(2,1)} %convolution_convert_fusion) | data formatting | bytes 8388608
  130.0 23.3 %reshape.292 = bf16[2048,1024]{1,0:T(8,128)(2,1)} reshape(bf16[2048,32,32]{2,1,0:T(8,128)(2,1)} %bitcast.96) | data formatting | bytes 8388608
  154.9 8.2 %reshape.291 = bf16[16,512,1,2,64]{4,3,1,0,2:T(2,128)(2,1)} reshape(bf16[8192,128]{1,0:T(8,128)(2,1)} %all-gather.4.cloned.1.call-done) | data formatting | bytes 4194304 | tf_op jit(solution)/shard_map/reshape | solution.py:47
  163.1 9.1 %copy.49 = bf16[16,512,1,2,64]{1,4,3,2,0:T(8,128)(2,1)S(1)} copy(bf16[16,512,1,2,64]{4,3,1,0,2:T(2,128)(2,1)} %reshape.291) | data formatting | bytes 4194304
  172.2 10.4 %all-gather.6.cloned.1.call-done = bf16[8192,128]{1,0:T(8,128)(2,1)} async-done(((bf16[1024,128]{1,0:T(8,128)(2,1)}), bf16[8192,128]{1,0:T(8,128)(2,1)}) %all-gather.6.cloned.1.call-update) | async-done | bytes 2097168 | tf_op jit(solution)/shard_map/all_gather | solution.py:22
  182.7 3.9 %copy.50 = bf16[16,512,1,128]{1,3,2,0:T(8,128)(2,1)} copy(bf16[16,512,1,128]{3,1,0,2:T(8,128)(2,1)} %bitcast.102) | data formatting | bytes 4194304
  186.7 24.3 %while.15 = (s32[]{:T(128)}, f32[256,1,2]{0,2,1:T(2,128)S(1)}, f32[256,1,2]{0,2,1:T(2,128)S(1)}, f32[256,1,2,128]{0,3,2,1:T(8,128)S(1)}, s32[16]{0:T(128)S(1)}, ...) while((s32[]{:T(128)}, f32[256,1,2]{0,2,1:T(2,128)S(1)}, ...), condition=%wide.region_5.6_spmd.clone, body=%wide.region_0.5_spmd.clone.sunk | while | flops 103287040 | bytes 4563285 | solution.py:84
  187.9 4.0 %conditional.3 = ((f32[256,1,2]{0,2,1:T(2,128)S(1)}, f32[256,1,2]{0,2,1:T(2,128)S(1)}, f32[256,1,2,128]{0,3,2,1:T(8,128)S(1)})) conditional(s32[]{:T(128)} %convert_element_type.74, (f32[256,1,2]{0,2,1:T(2,128)S(1)}, f32[256,1,2]{0,2,1:T(2,128)S(1)}, f32[256,1,2,128]{0,3,2,1:T(8,128)S(1)}) %tuple.42, (s32[]{:T(128)}, s32[]{:T(128)}, s32[]{:T(128)}, ...), branch_computations={%region_1.1_spmd, %region_2.4_spmd} | conditional | flops 103287040 | bytes 4562002 | solution.py:80
  212.2 11.2 %all-to-all-start = ((bf16[16,256,128]{1,2,0:T(8,128)(2,1)}), bf16[16,256,128]{1,2,0:T(8,128)(2,1)S(1)}, u32[]{:S(2)}, u32[]{:S(2)}) async-start(bf16[16,256,128]{1,2,0:T(8,128)(2,1)} %stack.3), calls=%async_computation | async-start | bytes 2097152 | tf_op jit(solution)/shard_map/all_to_all | solution.py:16
  223.6 45.2 %reduce-scatter.4.cloned.1.call-done = bf16[128,1024]{1,0:T(8,128)(2,1)} async-done(((bf16[2048,1024]{1,0:T(8,128)(2,1)}), bf16[128,1024]{1,0:T(8,128)(2,1)}) %reduce-scatter.4.cloned.1.call-update) | async-done | bytes 262160
  268.8 1.8 reshape.293
  270.7 1.8 copy.60
  272.5 44.5 %all-to-all-start.2 = ((bf16[32,32,128]{2,1,0:T(8,128)(2,1)}), bf16[32,32,128]{2,1,0:T(8,128)(2,1)S(1)}, u32[]{:S(2)}, u32[]{:S(2)}) async-start(bf16[32,32,128]{2,1,0:T(8,128)(2,1)} %copy.60), calls=%async_computation.2 | async-start | bytes 524288 | tf_op jit(solution)/shard_map/all_to_all | solution.py:145
  317.2 2.2 convolution_convert_fusion.1
  319.3 10.3 %all-to-all-done.2 = bf16[32,32,128]{2,1,0:T(8,128)(2,1)S(1)} async-done(((bf16[32,32,128]{2,1,0:T(8,128)(2,1)}), bf16[32,32,128]{2,1,0:T(8,128)(2,1)S(1)}, u32[]{:S(2)}, u32[]{:S(2)}) %all-to-all-start.2) | async-done | bytes 262176 | tf_op jit(solution)/shard_map/all_to_all | solution.py:145
  (127 shorter events, 24.6 us)
Async XLA Ops:
  7.2 96.6 %copy-start = (bf16[1,256,2048]{2,1,0:T(8,128)(2,1)S(1)}, bf16[1,256,2048]{2,1,0:T(8,128)(2,1)}, u32[]{:S(2)}) copy-start(bf16[1,256,2048]{2,1,0:T(8,128)(2,1)} %param.31) | copy-start | bytes 3145732
  7.2 91.6 %all-gather.8.cloned.1.call-start = ((), (), s32[]{:S(2)}) async-start(), calls=%async_computation.6 | async-start | bytes 4456448 | tf_op jit(solution)/shard_map/all_gather | solution.py:133
  16.5 32.0 %copy-start.2 = (bf16[256,128]{1,0:T(8,128)(2,1)S(1)}, bf16[256,128]{1,0:T(8,128)(2,1)}, u32[]{:S(2)}) copy-start(bf16[256,128]{1,0:T(8,128)(2,1)} %param.19) | copy-start | bytes 196612
  16.5 42.8 %copy-start.3 = (bf16[256,128]{1,0:T(8,128)(2,1)S(1)}, bf16[256,128]{1,0:T(8,128)(2,1)}, u32[]{:S(2)}) copy-start(bf16[256,128]{1,0:T(8,128)(2,1)} %param.20) | copy-start | bytes 196612
  16.5 82.3 %copy-start.8 = (bf16[1,2048,256]{2,1,0:T(8,128)(2,1)S(1)}, bf16[1,2048,256]{2,1,0:T(8,128)(2,1)}, u32[]{:S(2)}) copy-start(bf16[1,2048,256]{2,1,0:T(8,128)(2,1)} %param.29) | copy-start | bytes 3145732
  48.5 106.4 %all-gather.4.cloned.1.call-start = ((), (), s32[]{:S(2)}) async-start(), calls=%async_computation.4 | async-start | bytes 2359296 | tf_op jit(solution)/shard_map/all_gather | solution.py:22
  59.3 43.2 %copy-start.9 = (bf16[1,2048,256]{2,1,0:T(8,128)(2,1)S(1)}, bf16[1,2048,256]{2,1,0:T(8,128)(2,1)}, u32[]{:S(2)}) copy-start(bf16[1,2048,256]{2,1,0:T(8,128)(2,1)} %param.30) | copy-start | bytes 3145732
  59.3 123.4 %all-gather.6.cloned.1.call-start = ((), (), s32[]{:S(2)}) async-start(), calls=%async_computation.5 | async-start | bytes 2359296 | tf_op jit(solution)/shard_map/all_gather | solution.py:22
  70.5 198.3 %reduce-scatter.4.cloned.1.call-start = ((), (), s32[]{:S(2)}) async-start(), calls=%async_computation.7 | async-start | bytes 4456448
  98.8 3.6 %copy-start.7 = (bf16[32,32,2048]{2,1,0:T(8,128)(2,1)S(1)}, bf16[32,32,2048]{2,1,0:T(8,128)(2,1)}, u32[]{:S(2)}) copy-start(bf16[32,32,2048]{2,1,0:T(8,128)(2,1)} %all-gather.8.cloned.1.call-done) | copy-start | bytes 12582916
  153.3 0.8 copy-start.4
  186.7 24.4 %copy-start.6 = (f32[128]{0:T(128)S(1)}, f32[128]{0:T(128)}, u32[]{:S(2)}) copy-start(f32[128]{0:T(128)} %param.22) | copy-start | bytes 1540
  210.9 12.5 %copy-start.1 = (f32[256,8]{0,1:T(8,128)S(1)}, f32[256,8]{0,1:T(8,128)}, u32[]{:S(2)}) copy-start(f32[256,8]{0,1:T(8,128)} %param.27) | copy-start | bytes 24580
  210.9 12.5 %copy-start.5 = (f32[256,2]{0,1:T(2,128)S(1)}, f32[256,2]{0,1:T(2,128)}, u32[]{:S(2)}) copy-start(f32[256,2]{0,1:T(2,128)} %param.28) | copy-start | bytes 6148
  212.2 60.2 %all-to-all-start = ((bf16[16,256,128]{1,2,0:T(8,128)(2,1)}), bf16[16,256,128]{1,2,0:T(8,128)(2,1)S(1)}, u32[]{:S(2)}, u32[]{:S(2)}) async-start(bf16[16,256,128]{1,2,0:T(8,128)(2,1)} %stack.3), calls=%async_computation | async-start | bytes 2097152 | tf_op jit(solution)/shard_map/all_to_all | solution.py:16
  272.5 57.2 %all-to-all-start.2 = ((bf16[32,32,128]{2,1,0:T(8,128)(2,1)}), bf16[32,32,128]{2,1,0:T(8,128)(2,1)S(1)}, u32[]{:S(2)}, u32[]{:S(2)}) async-start(bf16[32,32,128]{2,1,0:T(8,128)(2,1)} %copy.60), calls=%async_computation.2 | async-start | bytes 524288 | tf_op jit(solution)/shard_map/all_to_all | solution.py:145
Sparse Core Ops, SparseCore 0:
  48.6 50.1 all-gather.7
  100.9 37.2 all-gather.3
  140.3 42.3 all-gather.5
  185.4 83.3 reduce-scatter.3
